TPU v7x, 512 devices: a whole 4x8x8 slice. The times are simulated.
512 devices in a mesh: ep: 128 (over z, y, core), tp: 4 (over x).
Axes of the slice: x: 4, y: 8, z: 8, core: 2. Of those that a mesh axis runs over, the one named last changes fastest.
Arguments:
- tokens: bfloat16 [1536, 1024], P('ep'), may hold values from -6 to 6
- attention_norm_gain: bfloat16 [1024], replicated, may hold values from 0.099609375 to 1.8984375
- query_weight: bfloat16 [1024, 1024], P('ep', 'tp'), may hold values from -0.3125 to 0.3125
- key_weight: bfloat16 [1024, 256], P('ep', 'tp'), may hold values from -0.1875 to 0.1875
- value_weight: bfloat16 [1024, 256], P('ep', 'tp'), may hold values from -0.1875 to 0.1875
- per_head_gain: bfloat16 [1024], P('tp'), may hold values from 0.099609375 to 1.8984375
- lambdas: float32 [8], replicated, may hold values from 0.3 to 0.8
- output_weight: bfloat16 [1024, 1024], P('tp'), may hold values from -0.1875 to 0.1875
- key_value_cache: bfloat16 [1536, 1024, 4, 128], P('ep', None, 'tp'), may hold values from -160 to 160, as said below
- lengths: int32 [1536], P('ep'), may hold values from 1 to 1023, as said below
- expert_norm_gain: bfloat16 [1024], replicated, may hold values from 0.099609375 to 1.8984375
- routes: int32 [1536, 6], P('ep'), may hold values from 0 to 127, all different within a row; in each aligned block of 12 rows (0 to 11, 12 to 23, ...) no two rows name the same one
- routing_weight: float32 [1536, 6], P('ep'), may hold values from 0.1 to 0.6
- expert_gate_weight: bfloat16 [128, 1024, 512], P('ep', None, 'tp'), may hold values from -0.1875 to 0.1875
- expert_up_weight: bfloat16 [128, 1024, 512], P('ep', None, 'tp'), may hold values from -0.1875 to 0.1875
- expert_down_weight: bfloat16 [128, 512, 1024], P('ep', 'tp'), may hold values from -0.25 to 0.25
- dense_gate_weight: bfloat16 [1024, 256], P('ep', 'tp'), may hold values from -0.1875 to 0.1875
- dense_up_weight: bfloat16 [1024, 256], P('ep', 'tp'), may hold values from -0.1875 to 0.1875
- dense_down_weight: bfloat16 [256, 1024], P('tp'), may hold values from -0.375 to 0.375
- dense_branch_gate: bfloat16 [1024], replicated, may hold values from -0.1875 to 0.1875
Outputs:
- mixed: bfloat16 [1536, 1024], P('ep', 'tp')
- new_rows: bfloat16 [1536, 4, 128], P('ep', 'tp')
Inputs may be any that keep to these rules, and one draw needn't show every extreme that they name: `key_value_cache`: cache positions at or beyond a sequence's length are never read. `lengths`: the number of cache positions already filled; the new token sits at that position; in each block of 12 sequences of one index of ep one sequence has 1023. `routes`: each row names 6 different experts; among the rows of one index of ep no expert is named more than 1 times, a bound that some block reaches.
All inputs are finite; a program needn't handle non-finite values.
Results may differ from a plain program's by a relative error of at most 0.015.
The roundings to bfloat16 on the way count: a program that leaves them out, or rounds other values in their place, can miss the bound.
Values may be sent and summed in bfloat16 or wider, within the bound.
A program may use at most 64 MiB of HBM per device.

v0:
```python
import jax
import jax.numpy as jnp
from jax import lax
from jax.sharding import Mesh
from jax.sharding import PartitionSpec as P

HD = 64
VD = 128
EP = ("ep_0", "ep_1", "ep_2")


epsilon = 1e-06


def sent_to_all(x, axis):
    copies = jnp.broadcast_to(x, (lax.axis_size(axis), *x.shape))
    return lax.all_to_all(copies, axis, split_axis=0, concat_axis=0, tiled=True)


def in_order(pieces, dim):
    pieces = jnp.moveaxis(pieces, 0, dim)
    dims = pieces.shape
    return pieces.reshape(*dims[:dim], dims[dim] * dims[dim + 1], *dims[dim + 2 :])


def gathered_by_axis(x, axes, dim):
    far, near = axes
    pieces = sent_to_all(sent_to_all(x, far), near)
    return in_order(pieces.swapaxes(0, 1).reshape(-1, *x.shape), dim)


def from_partner(block, axis, bit):
    count = lax.axis_size(axis)
    route = []
    for low in range(count):
        high = low | 1 << bit
        if high != low and high < count:
            route += [(low, high), (high, low)]
    return lax.ppermute(block, axis, route)


def over_copies(x, axis):
    return sent_to_all(x, axis).astype(jnp.float32).sum(axis=0)


def in_blocks(x, dim, count):
    dims = x.shape
    pieces = x.reshape(*dims[:dim], count, dims[dim] // count, *dims[dim + 1 :])
    return jnp.moveaxis(pieces, dim, 0)


def summed_on_arrival(x, axis, dim):
    count = lax.axis_size(axis)
    pieces = lax.all_to_all(in_blocks(x, dim, count), axis, 0, 0, tiled=True)
    return jnp.sum(pieces.astype(jnp.float32), axis=0)


def rms_scale(values, gain):
    mean_sq = jnp.mean(values * values, axis=-1, keepdims=True)
    return values * lax.rsqrt(mean_sq + epsilon) * gain.astype(jnp.float32)


def project(normed, weight):
    return jnp.dot(
        normed,
        gathered_by_axis(weight, (("ep_0", "ep_1"), "ep_2"), 0),
        preferred_element_type=jnp.float32,
    )


def map_weights(query, key_new, keys, seq_lengths):
    span = keys.shape[1]
    scale = query.shape[-1] ** (-0.5)
    scores = jnp.einsum("sugd,scud->sugc", query, keys, preferred_element_type=jnp.float32) * scale
    own = jnp.einsum("sugd,sud->sug", query, key_new, preferred_element_type=jnp.float32) * scale
    live = jnp.arange(span)[None, :] < seq_lengths[:, None]
    scores = jnp.where(live[:, None, None, :], scores, -jnp.inf)
    peak = jnp.maximum(jnp.max(scores, axis=-1), own)
    weights = jnp.exp(scores - peak[..., None])
    own_weight = jnp.exp(own - peak)
    total = jnp.sum(weights, axis=-1) + own_weight
    return (weights / total[..., None], own_weight / total)


def per_device(
    tokens,
    attention_norm_gain,
    query_weight,
    key_weight,
    value_weight,
    per_head_gain,
    lambdas,
    output_weight,
    key_value_cache,
    lengths,
    expert_norm_gain,
    routes,
    routing_weight,
    expert_gate_weight,
    expert_up_weight,
    expert_down_weight,
    dense_gate_weight,
    dense_up_weight,
    dense_down_weight,
    dense_branch_gate,
):
    sequences, model_width = tokens.shape
    units = key_value_cache.shape[2]
    lanes = key_value_cache.shape[3]
    normed = rms_scale(tokens.astype(jnp.float32), attention_norm_gain).astype(jnp.bfloat16)
    joined = jnp.concatenate([query_weight, key_weight, value_weight], axis=1)
    projected = project(normed, joined).astype(jnp.bfloat16)
    query_width = query_weight.shape[1]
    key_width = key_weight.shape[1]
    query = projected[:, :query_width].reshape(sequences, units, -1, HD)
    key_new = projected[:, query_width : query_width + key_width].reshape(sequences, units, HD)
    value_new = projected[:, query_width + key_width :].reshape(sequences, units, lanes - HD)
    weights, own_weight = map_weights(query, key_new, key_value_cache[..., :HD], lengths)
    members = lax.axis_size("tp")
    partner_bit = members.bit_length() - 2
    other, other_own = (
        from_partner(weights.astype(jnp.bfloat16), "tp", partner_bit).astype(weights.dtype),
        from_partner(own_weight.astype(jnp.bfloat16), "tp", partner_bit).astype(own_weight.dtype),
    )
    position = lax.axis_index("tp")
    first_map = position < members // 2
    kv_count = units * members // 2
    kv_ids = (position * units + jnp.arange(units, dtype=jnp.int32)) % kv_count
    table = lambdas.reshape(kv_count, -1)
    matches = kv_ids[:, None, None] == jnp.arange(kv_count, dtype=jnp.int32)[None, :, None]
    lam = jnp.sum(jnp.where(matches, table[None], 0.0), axis=1)
    leading = jnp.where(first_map, weights, other)
    trailing = jnp.where(first_map, other, weights)
    lead_own = jnp.where(first_map, own_weight, other_own)
    trail_own = jnp.where(first_map, other_own, own_weight)
    mixed_weights = (leading - lam[None, :, :, None] * trailing).astype(jnp.bfloat16)
    mixed_own = (lead_own - lam[None] * trail_own).astype(jnp.bfloat16)
    heads = jnp.einsum(
        "sugc,scuv->sugv",
        mixed_weights,
        key_value_cache[..., HD:],
        preferred_element_type=jnp.float32,
    )
    heads = (
        heads
        + mixed_own.astype(jnp.float32)[..., None] * value_new.astype(jnp.float32)[:, :, None, :]
    )
    squares = jnp.sum(heads * heads, axis=-1)
    partner_squares = from_partner(squares, "tp", partner_bit)
    scaling = lax.rsqrt((squares + partner_squares) / VD + epsilon)
    gain = per_head_gain.reshape(units, -1, lanes - HD).astype(jnp.float32)
    heads_normed = (heads * scaling[..., None] * gain[None]).astype(jnp.bfloat16)
    partial_value = jnp.dot(
        heads_normed.reshape(sequences, -1), output_weight, preferred_element_type=jnp.float32
    )
    attn_out = over_copies(partial_value.astype(jnp.bfloat16), "tp").astype(jnp.float32)
    resid = tokens.astype(jnp.float32) + attn_out
    normed_ffn = rms_scale(resid, expert_norm_gain).astype(jnp.bfloat16)
    dense_in = project(normed_ffn, jnp.concatenate([dense_gate_weight, dense_up_weight], axis=1))
    hidden_units = dense_gate_weight.shape[1]
    dense_hidden = (jax.nn.silu(dense_in[:, :hidden_units]) * dense_in[:, hidden_units:]).astype(
        jnp.bfloat16
    )
    dense_part = jnp.dot(dense_hidden, dense_down_weight, preferred_element_type=jnp.float32)
    dense_out = summed_on_arrival(dense_part.astype(jnp.bfloat16), "tp", 1)
    gate = jax.nn.sigmoid(
        jnp.dot(normed_ffn, dense_branch_gate, preferred_element_type=jnp.float32)
    )
    expert_count = lax.axis_size(EP)
    top_count = routes.shape[1]
    capacity = (sequences * top_count + expert_count - 1) // expert_count
    named = routes[:, :, None] == jnp.arange(expert_count, dtype=jnp.int32)[None, None, :]
    hits = jnp.sum(named.astype(jnp.int32), axis=1)
    before = jnp.cumsum(hits, axis=0) - hits
    slot_of = jnp.sum(jnp.where(named, before[:, None, :], 0), axis=2)
    placing = (hits[:, :, None] > 0) & (
        before[:, :, None] == jnp.arange(capacity, dtype=jnp.int32)[None, None, :]
    )
    outgoing = jnp.einsum(
        "sec,sd->ecd", placing.astype(jnp.bfloat16), normed_ffn, preferred_element_type=jnp.float32
    ).astype(jnp.bfloat16)
    arrived = lax.all_to_all(outgoing, EP, split_axis=0, concat_axis=0, tiled=True)
    sources, count, features = arrived.shape
    flattened_rows = arrived.reshape(sources * count, features)
    gate_part = jnp.dot(flattened_rows, expert_gate_weight[0], preferred_element_type=jnp.float32)
    up_projected = jnp.dot(flattened_rows, expert_up_weight[0], preferred_element_type=jnp.float32)
    inner = (jax.nn.silu(gate_part) * up_projected).astype(jnp.bfloat16)
    outcome = jnp.dot(inner, expert_down_weight[0], preferred_element_type=jnp.float32)
    quarter = summed_on_arrival(outcome.astype(jnp.bfloat16), "tp", 1).astype(jnp.bfloat16)
    quarter = quarter.reshape(sources, count, -1)
    answers = lax.all_to_all(quarter, EP, split_axis=0, concat_axis=0, tiled=True)
    quarter_width = answers.shape[2]
    answer_rows = answers.reshape(expert_count * capacity, quarter_width)
    picked = answer_rows[routes * capacity + slot_of]
    routed = jnp.sum(routing_weight[..., None] * picked.astype(jnp.float32), axis=1)
    column_start = lax.axis_index("tp") * quarter_width
    resid_part = lax.dynamic_slice_in_dim(resid, column_start, quarter_width, 1)
    mixed = (resid_part + routed + gate[:, None] * dense_out).astype(jnp.bfloat16)
    new_rows = jnp.concatenate([key_new, value_new], axis=2)
    return (mixed, new_rows)


def solution(mesh):
    split = Mesh(mesh.devices.reshape(8, 8, 2, mesh.shape["tp"]), ("ep_0", "ep_1", "ep_2", "tp"))
    return jax.shard_map(
        per_device,
        mesh=split,
        in_specs=(
            P(EP, None),
            P(),
            P(EP, "tp"),
            P(EP, "tp"),
            P(EP, "tp"),
            P("tp"),
            P(),
            P("tp", None),
            P(EP, None, "tp", None),
            P(EP),
            P(),
            P(EP, None),
            P(EP, None),
            P(EP, None, "tp"),
            P(EP, None, "tp"),
            P(EP, "tp", None),
            P(EP, "tp"),
            P(EP, "tp"),
            P("tp", None),
            P(),
        ),
        out_specs=(P(EP, "tp"), P(EP, "tp", None)),
        check_vma=False,
    )
```

profile of v0, /device:TPU:1, one launch (start us, length us, event | category | flops | bytes accessed | tf_op | source)
XLA Modules:
  0.0 160.1 jit_solution(17695869367653698291)
XLA Ops:
  0.7 0.9 pad_maximum_fusion
  1.5 0.8 broadcast_in_dim.49
  2.3 17.1 %all-to-all-start = ((bf16[64,8,384]{2,1,0:T(8,128)(2,1)}), bf16[64,8,384]{2,1,0:T(8,128)(2,1)S(1)}, u32[]{:S(2)}, u32[]{:S(2)}) async-start(bf16[64,8,384]{2,1,0:T(8,128)(2,1)} %broadcast_in_dim.49), calls=%async_computation | async-start | bytes 786432 | tf_op jit(solution)/shard_map/all_to_all | solution.py:17
  20.1 0.7 broadcast_in_dim_reshape.3
  20.9 0.7 reshape.227
  22.3 0.8 copy.97
  23.1 0.8 pad_maximum_fusion.2
  23.9 0.9 fusion.41
  24.9 0.7 iota_compare_fusion
  25.6 8.8 %all-to-all-done = bf16[64,8,384]{2,1,0:T(8,128)(2,1)S(1)} async-done(((bf16[64,8,384]{2,1,0:T(8,128)(2,1)}), bf16[64,8,384]{2,1,0:T(8,128)(2,1)S(1)}, u32[]{:S(2)}, u32[]{:S(2)}) %all-to-all-start) | async-done | bytes 393248 | tf_op jit(solution)/shard_map/all_to_all | solution.py:17
  34.6 7.2 %all_to_all.45 = bf16[2,64,8,384]{3,2,1,0:T(8,128)(2,1)S(1)} all-to-all(bf16[2,64,8,384]{3,2,1,0:T(8,128)(2,1)S(1)} %broadcast_in_dim.50), channel_id=1, replica_groups=mesh['ep_0'=8,'ep_1'=8,'ep_2'=2,'tp'=4] {'ep_2'}, dimensions={0} | all-to-all | bytes 1572864 | tf_op jit(solution)/shard_map/all_to_all | solution.py:17
  42.5 4.6 %all-to-all-start.6 = ((bf16[64,8,128]{2,1,0:T(8,128)(2,1)}), bf16[64,8,128]{2,1,0:T(8,128)(2,1)S(1)}, u32[]{:S(2)}, u32[]{:S(2)}) async-start(bf16[64,8,128]{2,1,0:T(8,128)(2,1)} %broadcast_in_dim.88), calls=%async_computation.6 | async-start | bytes 262144 | tf_op jit(solution)/shard_map/all_to_all | solution.py:17
  47.7 2.9 %fusion.78 = (f32[12,4]{1,0:T(8,128)S(1)}, f32[12,4,1024]{2,1,0:T(4,128)S(1)}) fusion(bf16[12,4,64]{2,1,0:T(4,128)(2,1)S(1)} %reshape.214, bf16[12,1024,1,128]{3,1,2,0:T(8,128)(2,1)} %param.28, pred[12,1024]{1,0:T(8,128)(4,1)S(1)} %iota_compare_fusion), kind=kOutput, calls=%fused_computation.112 | convolution fusion | flops 6438864 | bytes 3360960 | tf_op jit(solution)/shard_map/sugd,scud->sugc/dot_general | solution.py:74
  51.0 4.7 %collective-permute-start.1 = (bf16[12,1,4]{0,2,1:T(4,128)(2,1)S(1)}, bf16[12,1,4]{0,2,1:T(4,128)(2,1)S(1)}, u32[]{:S(2)}, u32[]{:S(2)}) collective-permute-start(bf16[12,1,4]{0,2,1:T(4,128)(2,1)S(1)} %bitcast.140), channel_id=1, source_target_pairs={{0,2},{2,0},{1,3},{3,1},{4,6},{6,4},{5,7},{7,5},{8,10},{10,8},{9,1... | collective-permute-start | bytes 296 | tf_op jit(solution)/shard_map/ppermute | solution.py:39
  55.9 2.1 %collective-permute-start = (bf16[12,1,4,1024]{3,2,0,1:T(4,128)(2,1)S(1)}, bf16[12,1,4,1024]{3,2,0,1:T(4,128)(2,1)S(1)}, u32[]{:S(2)}, u32[]{:S(2)}) collective-permute-start(bf16[12,1,4,1024]{3,2,0,1:T(4,128)(2,1)S(1)} %convert_bitcast_fusion), channel_id=1, source_target_pairs={{0,2},{2,0},{1,3},{3,1},{4,6},{6,4},{5,7},{7,5},{8,10},{10,8},{9,1... | collective-permute-start | bytes 294920 | tf_op jit(solution)/shard_map/ppermute | solution.py:39
  58.2 4.5 %collective-permute-done = bf16[12,1,4,1024]{3,2,0,1:T(4,128)(2,1)S(1)} collective-permute-done((bf16[12,1,4,1024]{3,2,0,1:T(4,128)(2,1)S(1)}, bf16[12,1,4,1024]{3,2,0,1:T(4,128)(2,1)S(1)}, u32[]{:S(2)}, u32[]{:S(2)}) %collective-permute-start) | collective-permute-done | bytes 98336 | tf_op jit(solution)/shard_map/ppermute | solution.py:39
  62.8 3.1 %multiply_reduce_fusion.2 = (f32[12,4]{1,0:T(8,128)S(1)}, f32[12,4,64]{2,1,0:T(4,128)S(1)}) fusion(f32[12,64]{1,0:T(8,128)S(1)} %get-tuple-element.9, f32[12,4]{1,0:T(8,128)S(1)} %copy.92, bf16[12,1024,1,128]{3,1,2,0:T(8,128)(2,1)} %param.28, bf16[12,1,4,1024]{3,2,0,1:T(4,128)(2,1)S(1)} %collective-permute-done, f32[4]{0:T(128)S(1)} %select_reduce_fusion.1, ...), kind=kOutput, calls=%fused_computation.70 | convolution fusion | flops 6696912 | bytes 3456785 | tf_op jit(solution)/shard_map/sugc,scuv->sugv/dot_general | solution.py:138
  66.0 2.3 %collective-permute-start.2 = (f32[12,1,4]{0,2,1:T(4,128)S(1)}, f32[12,1,4]{0,2,1:T(4,128)S(1)}, u32[]{:S(2)}, u32[]{:S(2)}) collective-permute-start(f32[12,1,4]{0,2,1:T(4,128)S(1)} %bitcast.139), channel_id=1, source_target_pairs={{0,2},{2,0},{1,3},{3,1},{4,6},{6,4},{5,7},{7,5},{8,10},{10,8},{9,1... | collective-permute-start | bytes 584 | tf_op jit(solution)/shard_map/ppermute | solution.py:39
  68.3 3.7 %collective-permute-done.2 = f32[12,1,4]{0,2,1:T(4,128)S(1)} collective-permute-done((f32[12,1,4]{0,2,1:T(4,128)S(1)}, f32[12,1,4]{0,2,1:T(4,128)S(1)}, u32[]{:S(2)}, u32[]{:S(2)}) %collective-permute-start.2) | collective-permute-done | bytes 224 | tf_op jit(solution)/shard_map/ppermute | solution.py:39
  73.1 3.3 %all-to-all-start.2 = ((bf16[4,12,1024]{2,1,0:T(8,128)(2,1)}), bf16[4,12,1024]{2,1,0:T(8,128)(2,1)S(1)}, u32[]{:S(2)}, u32[]{:S(2)}) async-start(bf16[4,12,1024]{2,1,0:T(8,128)(2,1)} %broadcast_in_dim.84), calls=%async_computation.2 | async-start | bytes 262144 | tf_op jit(solution)/shard_map/all_to_all | solution.py:17
  76.7 4.4 %all-to-all-done.2 = bf16[4,12,1024]{2,1,0:T(8,128)(2,1)S(1)} async-done(((bf16[4,12,1024]{2,1,0:T(8,128)(2,1)}), bf16[4,12,1024]{2,1,0:T(8,128)(2,1)S(1)}, u32[]{:S(2)}, u32[]{:S(2)}) %all-to-all-start.2) | async-done | bytes 98336 | tf_op jit(solution)/shard_map/all_to_all | solution.py:17
  81.9 7.5 %all-to-all-start.7 = ((bf16[2,64,8,128]{3,2,1,0:T(8,128)(2,1)}), bf16[2,64,8,128]{3,2,1,0:T(8,128)(2,1)S(1)}, u32[]{:S(2)}, u32[]{:S(2)}) async-start(bf16[2,64,8,128]{3,2,1,0:T(8,128)(2,1)} %broadcast_in_dim.89), calls=%async_computation.7 | async-start | bytes 524288 | tf_op jit(solution)/shard_map/all_to_all | solution.py:17
  90.5 0.8 reduce.8
  91.3 0.9 reshape.243
  92.1 13.1 %all-to-all-start.3 = ((bf16[128,2,512]{2,1,0:T(2,128)(2,1)}), bf16[128,2,512]{2,1,0:T(2,128)(2,1)S(1)}, u32[]{:S(2)}, u32[]{:S(2)}) async-start(bf16[128,2,512]{2,1,0:T(2,128)(2,1)} %reshape.243), calls=%async_computation.3 | async-start | bytes 524288 | tf_op jit(solution)/shard_map/all_to_all | solution.py:182
  105.7 14.8 %all-to-all-done.3 = bf16[128,2,512]{2,1,0:T(2,128)(2,1)S(1)} async-done(((bf16[128,2,512]{2,1,0:T(2,128)(2,1)}), bf16[128,2,512]{2,1,0:T(2,128)(2,1)S(1)}, u32[]{:S(2)}, u32[]{:S(2)}) %all-to-all-start.3) | async-done | bytes 262176 | tf_op jit(solution)/shard_map/all_to_all | solution.py:182
  122.1 3.4 %all-to-all-start.4 = ((bf16[4,128,256]{2,1,0:T(8,128)(2,1)}), bf16[4,128,256]{2,1,0:T(8,128)(2,1)S(1)}, u32[]{:S(2)}, u32[]{:S(2)}) async-start(bf16[4,128,256]{2,1,0:T(8,128)(2,1)} %bitcast.131), calls=%async_computation.4 | async-start | bytes 524288 | tf_op jit(solution)/shard_map/all_to_all | solution.py:54
  126.4 5.2 %all-to-all-done.4 = bf16[4,128,256]{2,1,0:T(8,128)(2,1)S(1)} async-done(((bf16[4,128,256]{2,1,0:T(8,128)(2,1)}), bf16[4,128,256]{2,1,0:T(8,128)(2,1)S(1)}, u32[]{:S(2)}, u32[]{:S(2)}) %all-to-all-start.4) | async-done | bytes 262176 | tf_op jit(solution)/shard_map/all_to_all | solution.py:54
  131.6 3.3 %all-to-all-start.8 = ((bf16[4,12,256]{2,1,0:T(8,128)(2,1)}), bf16[4,12,256]{2,1,0:T(8,128)(2,1)S(1)}, u32[]{:S(2)}, u32[]{:S(2)}) async-start(bf16[4,12,256]{2,1,0:T(8,128)(2,1)} %bitcast.133), calls=%async_computation.8 | async-start | bytes 65536 | tf_op jit(solution)/shard_map/all_to_all | solution.py:54
  136.9 2.2 %all-to-all-done.8 = bf16[4,12,256]{2,1,0:T(8,128)(2,1)S(1)} async-done(((bf16[4,12,256]{2,1,0:T(8,128)(2,1)}), bf16[4,12,256]{2,1,0:T(8,128)(2,1)S(1)}, u32[]{:S(2)}, u32[]{:S(2)}) %all-to-all-start.8) | async-done | bytes 24608 | tf_op jit(solution)/shard_map/all_to_all | solution.py:54
  139.1 7.8 %all-to-all-start.5 = ((bf16[128,2,128]{2,1,0:T(2,128)(2,1)}), bf16[128,2,128]{2,1,0:T(2,128)(2,1)S(1)}, u32[]{:S(2)}, u32[]{:S(2)}) async-start(bf16[128,2,128]{2,1,0:T(2,128)(2,1)} %reshape.245), calls=%async_computation.5 | async-start | bytes 131072 | tf_op jit(solution)/shard_map/all_to_all | solution.py:191
  147.1 11.4 %all-to-all-done.5 = bf16[128,2,128]{2,1,0:T(2,128)(2,1)S(1)} async-done(((bf16[128,2,128]{2,1,0:T(2,128)(2,1)}), bf16[128,2,128]{2,1,0:T(2,128)(2,1)S(1)}, u32[]{:S(2)}, u32[]{:S(2)}) %all-to-all-start.5) | async-done | bytes 65568 | tf_op jit(solution)/shard_map/all_to_all | solution.py:191
  (84 shorter events, 13.5 us)
Async XLA Ops:
  0.6 71.6 %copy-start = (bf16[256,1024]{1,0:T(8,128)(2,1)S(1)}, bf16[256,1024]{1,0:T(8,128)(2,1)}, u32[]{:S(2)}) copy-start(bf16[256,1024]{1,0:T(8,128)(2,1)} %param.27) | copy-start | bytes 1572868
  0.6 46.5 %copy-start.1 = (bf16[12,1024]{1,0:T(8,128)(2,1)S(1)}, bf16[12,1024]{1,0:T(8,128)(2,1)}, u32[]{:S(2)}) copy-start(bf16[12,1024]{1,0:T(8,128)(2,1)} %param.20) | copy-start | bytes 73732
  2.3 32.2 %all-to-all-start = ((bf16[64,8,384]{2,1,0:T(8,128)(2,1)}), bf16[64,8,384]{2,1,0:T(8,128)(2,1)S(1)}, u32[]{:S(2)}, u32[]{:S(2)}) async-start(bf16[64,8,384]{2,1,0:T(8,128)(2,1)} %broadcast_in_dim.49), calls=%async_computation | async-start | bytes 786432 | tf_op jit(solution)/shard_map/all_to_all | solution.py:17
  42.5 30.0 %all-to-all-start.6 = ((bf16[64,8,128]{2,1,0:T(8,128)(2,1)}), bf16[64,8,128]{2,1,0:T(8,128)(2,1)S(1)}, u32[]{:S(2)}, u32[]{:S(2)}) async-start(bf16[64,8,128]{2,1,0:T(8,128)(2,1)} %broadcast_in_dim.88), calls=%async_computation.6 | async-start | bytes 262144 | tf_op jit(solution)/shard_map/all_to_all | solution.py:17
  51.0 7.1 %collective-permute-start.1 = (bf16[12,1,4]{0,2,1:T(4,128)(2,1)S(1)}, bf16[12,1,4]{0,2,1:T(4,128)(2,1)S(1)}, u32[]{:S(2)}, u32[]{:S(2)}) collective-permute-start(bf16[12,1,4]{0,2,1:T(4,128)(2,1)S(1)} %bitcast.140), channel_id=1, source_target_pairs={{0,2},{2,0},{1,3},{3,1},{4,6},{6,4},{5,7},{7,5},{8,10},{10,8},{9,1... | collective-permute-start | bytes 296 | tf_op jit(solution)/shard_map/ppermute | solution.py:39
  55.9 6.9 %collective-permute-start = (bf16[12,1,4,1024]{3,2,0,1:T(4,128)(2,1)S(1)}, bf16[12,1,4,1024]{3,2,0,1:T(4,128)(2,1)S(1)}, u32[]{:S(2)}, u32[]{:S(2)}) collective-permute-start(bf16[12,1,4,1024]{3,2,0,1:T(4,128)(2,1)S(1)} %convert_bitcast_fusion), channel_id=1, source_target_pairs={{0,2},{2,0},{1,3},{3,1},{4,6},{6,4},{5,7},{7,5},{8,10},{10,8},{9,1... | collective-permute-start | bytes 294920 | tf_op jit(solution)/shard_map/ppermute | solution.py:39
  65.9 39.5 %copy-start.6 = (f32[12,6]{0,1:T(8,128)S(1)}, f32[12,6]{0,1:T(8,128)}, u32[]{:S(2)}) copy-start(f32[12,6]{0,1:T(8,128)} %param.32) | copy-start | bytes 868
  65.9 39.6 %copy-start.7 = (bf16[1024]{0:T(1024)(128)(2,1)S(1)}, bf16[1024]{0:T(1024)(128)(2,1)}, u32[]{:S(2)}) copy-start(bf16[1024]{0:T(1024)(128)(2,1)} %param.39) | copy-start | bytes 6148
  65.9 54.9 %copy-start.4 = (bf16[1,1024,128]{2,1,0:T(8,128)(2,1)S(1)}, bf16[1,1024,128]{2,1,0:T(8,128)(2,1)}, u32[]{:S(2)}) copy-start(bf16[1,1024,128]{2,1,0:T(8,128)(2,1)} %param.33) | copy-start | bytes 786436
  66.0 6.0 %collective-permute-start.2 = (f32[12,1,4]{0,2,1:T(4,128)S(1)}, f32[12,1,4]{0,2,1:T(4,128)S(1)}, u32[]{:S(2)}, u32[]{:S(2)}) collective-permute-start(f32[12,1,4]{0,2,1:T(4,128)S(1)} %bitcast.139), channel_id=1, source_target_pairs={{0,2},{2,0},{1,3},{3,1},{4,6},{6,4},{5,7},{7,5},{8,10},{10,8},{9,1... | collective-permute-start | bytes 584 | tf_op jit(solution)/shard_map/ppermute | solution.py:39
  72.2 48.8 %copy-start.2 = (bf16[1,128,1024]{2,1,0:T(8,128)(2,1)S(1)}, bf16[1,128,1024]{2,1,0:T(8,128)(2,1)}, u32[]{:S(2)}) copy-start(bf16[1,128,1024]{2,1,0:T(8,128)(2,1)} %param.35) | copy-start | bytes 786436
  72.2 48.8 %copy-start.3 = (bf16[1,1024,128]{2,1,0:T(8,128)(2,1)S(1)}, bf16[1,1024,128]{2,1,0:T(8,128)(2,1)}, u32[]{:S(2)}) copy-start(bf16[1,1024,128]{2,1,0:T(8,128)(2,1)} %param.34) | copy-start | bytes 786436
  73.1 8.1 %all-to-all-start.2 = ((bf16[4,12,1024]{2,1,0:T(8,128)(2,1)}), bf16[4,12,1024]{2,1,0:T(8,128)(2,1)S(1)}, u32[]{:S(2)}, u32[]{:S(2)}) async-start(bf16[4,12,1024]{2,1,0:T(8,128)(2,1)} %broadcast_in_dim.84), calls=%async_computation.2 | async-start | bytes 262144 | tf_op jit(solution)/shard_map/all_to_all | solution.py:17
  81.9 10.2 %all-to-all-start.7 = ((bf16[2,64,8,128]{3,2,1,0:T(8,128)(2,1)}), bf16[2,64,8,128]{3,2,1,0:T(8,128)(2,1)S(1)}, u32[]{:S(2)}, u32[]{:S(2)}) async-start(bf16[2,64,8,128]{3,2,1,0:T(8,128)(2,1)} %broadcast_in_dim.89), calls=%async_computation.7 | async-start | bytes 524288 | tf_op jit(solution)/shard_map/all_to_all | solution.py:17
  89.7 35.9 %copy-start.5 = (bf16[64,1024]{1,0:T(8,128)(2,1)S(1)}, bf16[64,1024]{1,0:T(8,128)(2,1)}, u32[]{:S(2)}) copy-start(bf16[64,1024]{1,0:T(8,128)(2,1)} %param.38) | copy-start | bytes 393220
  92.1 28.4 %all-to-all-start.3 = ((bf16[128,2,512]{2,1,0:T(2,128)(2,1)}), bf16[128,2,512]{2,1,0:T(2,128)(2,1)S(1)}, u32[]{:S(2)}, u32[]{:S(2)}) async-start(bf16[128,2,512]{2,1,0:T(2,128)(2,1)} %reshape.243), calls=%async_computation.3 | async-start | bytes 524288 | tf_op jit(solution)/shard_map/all_to_all | solution.py:182
  122.1 9.5 %all-to-all-start.4 = ((bf16[4,128,256]{2,1,0:T(8,128)(2,1)}), bf16[4,128,256]{2,1,0:T(8,128)(2,1)S(1)}, u32[]{:S(2)}, u32[]{:S(2)}) async-start(bf16[4,128,256]{2,1,0:T(8,128)(2,1)} %bitcast.131), calls=%async_computation.4 | async-start | bytes 524288 | tf_op jit(solution)/shard_map/all_to_all | solution.py:54
  131.6 7.5 %all-to-all-start.8 = ((bf16[4,12,256]{2,1,0:T(8,128)(2,1)}), bf16[4,12,256]{2,1,0:T(8,128)(2,1)S(1)}, u32[]{:S(2)}, u32[]{:S(2)}) async-start(bf16[4,12,256]{2,1,0:T(8,128)(2,1)} %bitcast.133), calls=%async_computation.8 | async-start | bytes 65536 | tf_op jit(solution)/shard_map/all_to_all | solution.py:54
  139.1 19.4 %all-to-all-start.5 = ((bf16[128,2,128]{2,1,0:T(2,128)(2,1)}), bf16[128,2,128]{2,1,0:T(2,128)(2,1)S(1)}, u32[]{:S(2)}, u32[]{:S(2)}) async-start(bf16[128,2,128]{2,1,0:T(2,128)(2,1)} %reshape.245), calls=%async_computation.5 | async-start | bytes 131072 | tf_op jit(solution)/shard_map/all_to_all | solution.py:191
where the time goes:
time: 161 us; the launch traced here: 160 us
  starting transfers between devices  69.3 us (43%)
  waiting for transfers between devices  55.2 us (34%)
  local copies, waits for them, and re-layouts  10.5 us (7%)
  other arithmetic  9.05 us (6%)
  matrix products  7.88 us (5%)
  blocking collectives  7.24 us (4%)
    all_to_all x4, starting transfers between devices, sent_to_all(): return lax.all_to_all(copies, axis, split_axis=0, concat_axis=0, tiled=True)  32.6 us
    all_to_all x1, waiting for transfers between devices, per_device(): lax.all_to_all(outgoing, EP, split_axis=0, concat_axis=0, tiled=True)  14.8 us
    all_to_all x4, waiting for transfers between devices, sent_to_all(): return lax.all_to_all(copies, axis, split_axis=0, concat_axis=0, tiled=True)  13.3 us
    all_to_all x1, starting transfers between devices, per_device(): lax.all_to_all(outgoing, EP, split_axis=0, concat_axis=0, tiled=True)  13.1 us
    all_to_all x1, waiting for transfers between devices, per_device(): lax.all_to_all(quarter, EP, split_axis=0, concat_axis=0, tiled=True)  11.4 us
    ppermute x3, starting transfers between devices, from_partner(): return lax.ppermute(block, axis, route)  9.05 us
    ppermute x3, waiting for transfers between devices, from_partner(): return lax.ppermute(block, axis, route)  8.2 us
    all_to_all x1, starting transfers between devices, per_device(): lax.all_to_all(quarter, EP, split_axis=0, concat_axis=0, tiled=True)  7.84 us
  transfers between devices with their start and end apart: 11, of which 8 were waited for; matrix products, arithmetic and copies ran while one was open for 13% of the time, Pallas kernels for 0%

commit v1 on v0

--- a/solution.py
+++ b/solution.py
@@ -1,6 +1,10 @@
+import functools
+
 import jax
 import jax.numpy as jnp
 from jax import lax
+from jax.experimental import pallas as pl
+from jax.experimental.pallas import tpu as pltpu
 from jax.sharding import Mesh
 from jax.sharding import PartitionSpec as P
 
@@ -53,6 +57,57 @@
     count = lax.axis_size(axis)
     pieces = lax.all_to_all(in_blocks(x, dim, count), axis, 0, 0, tiled=True)
     return jnp.sum(pieces.astype(jnp.float32), axis=0)
+
+
+MESH_ID = pl.DeviceIdType.MESH
+
+
+def exchange_kernel(nz, ny, nc, src, dst, send_sem, recv_sem):
+    z, y, c = (lax.axis_index(name) for name in EP)
+    x = lax.axis_index("tp")
+    count = nz * ny * nc
+    me = (z * ny + y) * nc + c
+
+    def peer(k):
+        i, j, dc = k // (ny * nc), (k // nc) % ny, k % nc
+        dz = nz // 2 + (1 - 2 * (i % 2)) * ((i + 1) // 2)
+        dy = ny // 2 + (1 - 2 * (j % 2)) * ((j + 1) // 2)
+        z2, y2, c2 = (z + dz) % nz, (y + dy) % ny, (c + dc + 1) % nc
+        return (z2 * ny + y2) * nc + c2, (z2, y2, c2, x)
+
+    barrier = pltpu.get_barrier_semaphore()
+
+    def greet(k, carry):
+        pl.semaphore_signal(barrier, inc=1, device_id=peer(k)[1], device_id_type=MESH_ID)
+        return carry
+
+    lax.fori_loop(0, count - 1, greet, 0)
+    dst[me] = src[me]
+    pl.semaphore_wait(barrier, count - 1)
+
+    def send(k, carry):
+        other, device = peer(k)
+        pltpu.make_async_remote_copy(
+            src.at[other], dst.at[me], send_sem, recv_sem, device_id=device, device_id_type=MESH_ID
+        ).start()
+        return carry
+
+    lax.fori_loop(0, count - 1, send, 0)
+    rest = pl.ds(0, count - 1)
+    pltpu.make_async_copy(src.at[rest], dst.at[rest], recv_sem).wait()
+    pltpu.make_async_copy(src.at[rest], dst.at[rest], send_sem).wait()
+
+
+def exchange(rows, collective_id):
+    nz, ny, nc = (lax.axis_size(name) for name in EP)
+    return pl.pallas_call(
+        functools.partial(exchange_kernel, nz, ny, nc),
+        out_shape=jax.ShapeDtypeStruct(rows.shape, rows.dtype),
+        in_specs=[pl.BlockSpec(memory_space=pltpu.VMEM)],
+        out_specs=pl.BlockSpec(memory_space=pltpu.VMEM),
+        scratch_shapes=[pltpu.SemaphoreType.DMA, pltpu.SemaphoreType.DMA],
+        compiler_params=pltpu.CompilerParams(collective_id=collective_id, has_side_effects=True),
+    )(rows)
 
 
 def rms_scale(values, gain):
@@ -179,7 +234,7 @@
     outgoing = jnp.einsum(
         "sec,sd->ecd", placing.astype(jnp.bfloat16), normed_ffn, preferred_element_type=jnp.float32
     ).astype(jnp.bfloat16)
-    arrived = lax.all_to_all(outgoing, EP, split_axis=0, concat_axis=0, tiled=True)
+    arrived = exchange(outgoing.reshape(expert_count, 8, -1), 0).reshape(outgoing.shape)
     sources, count, features = arrived.shape
     flattened_rows = arrived.reshape(sources * count, features)
     gate_part = jnp.dot(flattened_rows, expert_gate_weight[0], preferred_element_type=jnp.float32)
@@ -188,7 +243,7 @@
     outcome = jnp.dot(inner, expert_down_weight[0], preferred_element_type=jnp.float32)
     quarter = summed_on_arrival(outcome.astype(jnp.bfloat16), "tp", 1).astype(jnp.bfloat16)
     quarter = quarter.reshape(sources, count, -1)
-    answers = lax.all_to_all(quarter, EP, split_axis=0, concat_axis=0, tiled=True)
+    answers = exchange(quarter.reshape(expert_count, 2, -1), 1).reshape(quarter.shape)
     quarter_width = answers.shape[2]
     answer_rows = answers.reshape(expert_count * capacity, quarter_width)
     picked = answer_rows[routes * capacity + slot_of]

time: 161 us -> 153 us (0.950)
  Pallas kernels: 0 us -> 45.7 us
  waiting for transfers between devices: 55.2 us -> 21 us
  starting transfers between devices: 69.3 us -> 42.5 us
  blocking collectives: 7.24 us -> 12.9 us
  matrix products: 7.88 us -> 9.76 us
    pallas_call x0 -> x2, Pallas kernels: none -> 45.7 us  [exchange(): pl.pallas_call(functools.partial(exchange_kernel, nz, ny, nc), out_shape=...]
    all_to_all x2 -> x0, waiting for transfers between devices: 26.2 us -> none  [the longest x1 14.8 us: per_device(): lax.all_to_all(outgoing, EP, split_axis=0, concat_axis=0, tiled=True)]
    all_to_all x2 -> x0, starting transfers between devices: 21 us -> none  [the longest x1 13.1 us: per_device(): lax.all_to_all(outgoing, EP, split_axis=0, concat_axis=0, tiled=True)]
    all_to_all x4 -> x3, starting transfers between devices: 32.6 us -> 25.8 us  [sent_to_all(): return lax.all_to_all(copies, axis, split_axis=0, concat_axis=0, tiled=True)]
    all_to_all x1 -> x2, blocking collectives: 7.24 us -> 12.9 us  [sent_to_all(): return lax.all_to_all(copies, axis, split_axis=0, concat_axis=0, tiled=True)]
    ppermute x3, waiting for transfers between devices: 8.2 us -> 4.55 us  [from_partner(): return lax.ppermute(block, axis, route)]
    all_to_all x4 -> x3, waiting for transfers between devices: 13.3 us -> 11 us  [sent_to_all(): return lax.all_to_all(copies, axis, split_axis=0, concat_axis=0, tiled=True)]
    all_to_all x2, waiting for transfers between devices: 7.46 us -> 5.4 us  [summed_on_arrival(): pieces = lax.all_to_all(in_blocks(x, dim, count), axis, 0, 0, tiled=True)]
  transfers between devices with their start and end apart: 11 -> 8, of which waited for: 8 -> 4; matrix products, arithmetic and copies ran while one was open for 13% -> 13% of each run, Pallas kernels for 0% -> 17%
where the time goes in v1:
time: 153 us; the launch traced here: 152 us
  Pallas kernels  45.7 us (30%)
  starting transfers between devices  42.5 us (28%)
  waiting for transfers between devices  21 us (14%)
  blocking collectives  12.9 us (8%)
  local copies, waits for them, and re-layouts  11.1 us (7%)
  matrix products  9.76 us (6%)
  other arithmetic  7.61 us (5%)
    pallas_call x2, Pallas kernels, exchange(): pl.pallas_call(functools.partial(exchange_kernel, nz, ny, nc), out_shape=...  45.7 us
    all_to_all x3, starting transfers between devices, sent_to_all(): return lax.all_to_all(copies, axis, split_axis=0, concat_axis=0, tiled=True)  25.8 us
    all_to_all x2, blocking collectives, sent_to_all(): return lax.all_to_all(copies, axis, split_axis=0, concat_axis=0, tiled=True)  12.9 us
    all_to_all x3, waiting for transfers between devices, sent_to_all(): return lax.all_to_all(copies, axis, split_axis=0, concat_axis=0, tiled=True)  11 us
    ppermute x3, starting transfers between devices, from_partner(): return lax.ppermute(block, axis, route)  9.04 us
    all_to_all x2, starting transfers between devices, summed_on_arrival(): pieces = lax.all_to_all(in_blocks(x, dim, count), axis, 0, 0, tiled=True)  7.74 us
    all_to_all x2, waiting for transfers between devices, summed_on_arrival(): pieces = lax.all_to_all(in_blocks(x, dim, count), axis, 0, 0, tiled=True)  5.4 us
    ppermute x3, waiting for transfers between devices, from_partner(): return lax.ppermute(block, axis, route)  4.55 us
  transfers between devices with their start and end apart: 8, of which 4 were waited for; matrix products, arithmetic and copies ran while one was open for 13% of the time, Pallas kernels for 17%

profile of v1, /device:TPU:1, one launch (start us, length us, event | category | flops | bytes accessed | tf_op | source)
XLA Modules:
  0.0 151.6 jit_solution(17671140449880344054)
XLA Ops:
  0.7 0.9 pad_maximum_fusion
  1.5 0.8 broadcast_in_dim.49
  2.3 17.1 %all-to-all-start = ((bf16[64,8,384]{2,1,0:T(8,128)(2,1)}), bf16[64,8,384]{2,1,0:T(8,128)(2,1)S(1)}, u32[]{:S(2)}, u32[]{:S(2)}) async-start(bf16[64,8,384]{2,1,0:T(8,128)(2,1)} %broadcast_in_dim.49), calls=%async_computation | async-start | bytes 786432 | tf_op jit(solution)/shard_map/all_to_all | solution.py:21
  20.1 0.7 broadcast_in_dim_reshape.3
  20.9 0.7 reshape.220
  22.3 0.8 copy.78
  23.6 0.8 copy.77
  25.1 0.8 pad_maximum_fusion.2
  26.0 0.9 fusion.41
  26.9 0.7 iota_compare_fusion
  27.6 6.9 %all-to-all-done = bf16[64,8,384]{2,1,0:T(8,128)(2,1)S(1)} async-done(((bf16[64,8,384]{2,1,0:T(8,128)(2,1)}), bf16[64,8,384]{2,1,0:T(8,128)(2,1)S(1)}, u32[]{:S(2)}, u32[]{:S(2)}) %all-to-all-start) | async-done | bytes 393248 | tf_op jit(solution)/shard_map/all_to_all | solution.py:21
  34.6 7.2 %all_to_all.35 = bf16[2,64,8,384]{3,2,1,0:T(8,128)(2,1)S(1)} all-to-all(bf16[2,64,8,384]{3,2,1,0:T(8,128)(2,1)S(1)} %broadcast_in_dim.50), channel_id=1, replica_groups=mesh['ep_0'=8,'ep_1'=8,'ep_2'=2,'tp'=4] {'ep_2'}, dimensions={0} | all-to-all | bytes 1572864 | tf_op jit(solution)/shard_map/all_to_all | solution.py:21
  42.5 4.6 %all-to-all-start.4 = ((bf16[64,8,128]{2,1,0:T(8,128)(2,1)}), bf16[64,8,128]{2,1,0:T(8,128)(2,1)S(1)}, u32[]{:S(2)}, u32[]{:S(2)}) async-start(bf16[64,8,128]{2,1,0:T(8,128)(2,1)} %broadcast_in_dim.88), calls=%async_computation.4 | async-start | bytes 262144 | tf_op jit(solution)/shard_map/all_to_all | solution.py:21
  47.7 2.9 %fusion.78 = (f32[12,4]{1,0:T(8,128)S(1)}, f32[12,4,1024]{2,1,0:T(4,128)S(1)}) fusion(bf16[12,4,64]{2,1,0:T(4,128)(2,1)S(1)} %reshape.209, bf16[12,1024,1,128]{3,1,2,0:T(8,128)(2,1)} %param.28, pred[12,1024]{1,0:T(8,128)(4,1)S(1)} %iota_compare_fusion), kind=kOutput, calls=%fused_computation.112 | convolution fusion | flops 6438864 | bytes 3360960 | tf_op jit(solution)/shard_map/sugd,scud->sugc/dot_general | solution.py:129
  51.0 4.7 %collective-permute-start.1 = (bf16[12,1,4]{0,2,1:T(4,128)(2,1)S(1)}, bf16[12,1,4]{0,2,1:T(4,128)(2,1)S(1)}, u32[]{:S(2)}, u32[]{:S(2)}) collective-permute-start(bf16[12,1,4]{0,2,1:T(4,128)(2,1)S(1)} %bitcast.145), channel_id=1, source_target_pairs={{0,2},{2,0},{1,3},{3,1},{4,6},{6,4},{5,7},{7,5},{8,10},{10,8},{9,1... | collective-permute-start | bytes 296 | tf_op jit(solution)/shard_map/ppermute | solution.py:43
  55.9 2.1 %collective-permute-start = (bf16[12,1,4,1024]{3,2,0,1:T(4,128)(2,1)S(1)}, bf16[12,1,4,1024]{3,2,0,1:T(4,128)(2,1)S(1)}, u32[]{:S(2)}, u32[]{:S(2)}) collective-permute-start(bf16[12,1,4,1024]{3,2,0,1:T(4,128)(2,1)S(1)} %convert_bitcast_fusion), channel_id=1, source_target_pairs={{0,2},{2,0},{1,3},{3,1},{4,6},{6,4},{5,7},{7,5},{8,10},{10,8},{9,1... | collective-permute-start | bytes 294920 | tf_op jit(solution)/shard_map/ppermute | solution.py:43
  58.2 4.5 %collective-permute-done = bf16[12,1,4,1024]{3,2,0,1:T(4,128)(2,1)S(1)} collective-permute-done((bf16[12,1,4,1024]{3,2,0,1:T(4,128)(2,1)S(1)}, bf16[12,1,4,1024]{3,2,0,1:T(4,128)(2,1)S(1)}, u32[]{:S(2)}, u32[]{:S(2)}) %collective-permute-start) | collective-permute-done | bytes 98336 | tf_op jit(solution)/shard_map/ppermute | solution.py:43
  62.8 3.1 %multiply_reduce_fusion.2 = (f32[12,4]{1,0:T(8,128)S(1)}, f32[12,4,64]{2,1,0:T(4,128)S(1)}) fusion(f32[12,64]{1,0:T(8,128)S(1)} %get-tuple-element.9, f32[12,4]{1,0:T(8,128)S(1)} %copy.73, bf16[12,1024,1,128]{3,1,2,0:T(8,128)(2,1)} %param.28, bf16[12,1,4,1024]{3,2,0,1:T(4,128)(2,1)S(1)} %collective-permute-done, f32[4]{0:T(128)S(1)} %select_reduce_fusion.1, ...), kind=kOutput, calls=%fused_computation.70 | convolution fusion | flops 6696912 | bytes 3456785 | tf_op jit(solution)/shard_map/sugc,scuv->sugv/dot_general | solution.py:193
  66.0 2.3 %collective-permute-start.2 = (f32[12,1,4]{0,2,1:T(4,128)S(1)}, f32[12,1,4]{0,2,1:T(4,128)S(1)}, u32[]{:S(2)}, u32[]{:S(2)}) collective-permute-start(f32[12,1,4]{0,2,1:T(4,128)S(1)} %bitcast.144), channel_id=1, source_target_pairs={{0,2},{2,0},{1,3},{3,1},{4,6},{6,4},{5,7},{7,5},{8,10},{10,8},{9,1... | collective-permute-start | bytes 584 | tf_op jit(solution)/shard_map/ppermute | solution.py:43
  68.3 5.7 %all_to_all.36 = bf16[2,64,8,128]{3,2,1,0:T(8,128)(2,1)S(1)} all-to-all(bf16[2,64,8,128]{3,2,1,0:T(8,128)(2,1)S(1)} %broadcast_in_dim.89), channel_id=1, replica_groups=mesh['ep_0'=8,'ep_1'=8,'ep_2'=2,'tp'=4] {'ep_2'}, dimensions={0} | all-to-all | bytes 524288 | tf_op jit(solution)/shard_map/all_to_all | solution.py:21
  75.1 4.0 %all-to-all-start.2 = ((bf16[4,12,1024]{2,1,0:T(8,128)(2,1)}), bf16[4,12,1024]{2,1,0:T(8,128)(2,1)S(1)}, u32[]{:S(2)}, u32[]{:S(2)}) async-start(bf16[4,12,1024]{2,1,0:T(8,128)(2,1)} %broadcast_in_dim.84), calls=%async_computation.2 | async-start | bytes 262144 | tf_op jit(solution)/shard_map/all_to_all | solution.py:21
  79.8 4.2 %all-to-all-done.2 = bf16[4,12,1024]{2,1,0:T(8,128)(2,1)S(1)} async-done(((bf16[4,12,1024]{2,1,0:T(8,128)(2,1)}), bf16[4,12,1024]{2,1,0:T(8,128)(2,1)S(1)}, u32[]{:S(2)}, u32[]{:S(2)}) %all-to-all-start.2) | async-done | bytes 98336 | tf_op jit(solution)/shard_map/all_to_all | solution.py:21
  85.5 3.3 %all-to-all-start.6 = ((bf16[4,12,256]{2,1,0:T(8,128)(2,1)}), bf16[4,12,256]{2,1,0:T(8,128)(2,1)S(1)}, u32[]{:S(2)}, u32[]{:S(2)}) async-start(bf16[4,12,256]{2,1,0:T(8,128)(2,1)} %bitcast.135), calls=%async_computation.6 | async-start | bytes 65536 | tf_op jit(solution)/shard_map/all_to_all | solution.py:58
  88.8 0.7 copy.89
  89.5 25.5 %shard_map.203 = bf16[128,8,128]{2,1,0:T(8,128)(2,1)} custom-call(bf16[128,8,128]{2,1,0:T(8,128)(2,1)} %bitcast.142), custom_call_target="tpu_custom_call" | custom-call | tf_op jit(solution)/shard_map/pallas_call | solution.py:103
  115.0 1.2 fusion.23
  116.2 1.3 convolution_convert_fusion
  118.3 4.5 %all-to-all-start.3 = ((bf16[4,128,256]{2,1,0:T(8,128)(2,1)}), bf16[4,128,256]{2,1,0:T(8,128)(2,1)S(1)}, u32[]{:S(2)}, u32[]{:S(2)}) async-start(bf16[4,128,256]{2,1,0:T(8,128)(2,1)} %bitcast.133), calls=%async_computation.3 | async-start | bytes 524288 | tf_op jit(solution)/shard_map/all_to_all | solution.py:58
  122.9 5.4 %all-to-all-done.3 = bf16[4,128,256]{2,1,0:T(8,128)(2,1)S(1)} async-done(((bf16[4,128,256]{2,1,0:T(8,128)(2,1)}), bf16[4,128,256]{2,1,0:T(8,128)(2,1)S(1)}, u32[]{:S(2)}, u32[]{:S(2)}) %all-to-all-start.3) | async-done | bytes 262176 | tf_op jit(solution)/shard_map/all_to_all | solution.py:58
  129.0 20.2 %shard_map.204 = bf16[128,2,128]{2,1,0:T(2,128)(2,1)} custom-call(bf16[128,2,128]{2,1,0:T(2,128)(2,1)} %reshape_reshape.17.src), custom_call_target="tpu_custom_call" | custom-call | tf_op jit(solution)/shard_map/pallas_call | solution.py:103
  149.2 0.9 copy.125
  150.0 0.7 gather_fusion
  (72 shorter events, 10.7 us)
Async XLA Ops:
  0.6 73.7 %copy-start = (bf16[256,1024]{1,0:T(8,128)(2,1)S(1)}, bf16[256,1024]{1,0:T(8,128)(2,1)}, u32[]{:S(2)}) copy-start(bf16[256,1024]{1,0:T(8,128)(2,1)} %param.27) | copy-start | bytes 1572868
  0.6 46.5 %copy-start.1 = (bf16[12,1024]{1,0:T(8,128)(2,1)S(1)}, bf16[12,1024]{1,0:T(8,128)(2,1)}, u32[]{:S(2)}) copy-start(bf16[12,1024]{1,0:T(8,128)(2,1)} %param.20) | copy-start | bytes 73732
  2.3 32.2 %all-to-all-start = ((bf16[64,8,384]{2,1,0:T(8,128)(2,1)}), bf16[64,8,384]{2,1,0:T(8,128)(2,1)S(1)}, u32[]{:S(2)}, u32[]{:S(2)}) async-start(bf16[64,8,384]{2,1,0:T(8,128)(2,1)} %broadcast_in_dim.49), calls=%async_computation | async-start | bytes 786432 | tf_op jit(solution)/shard_map/all_to_all | solution.py:21
  42.5 25.8 %all-to-all-start.4 = ((bf16[64,8,128]{2,1,0:T(8,128)(2,1)}), bf16[64,8,128]{2,1,0:T(8,128)(2,1)S(1)}, u32[]{:S(2)}, u32[]{:S(2)}) async-start(bf16[64,8,128]{2,1,0:T(8,128)(2,1)} %broadcast_in_dim.88), calls=%async_computation.4 | async-start | bytes 262144 | tf_op jit(solution)/shard_map/all_to_all | solution.py:21
  51.0 7.1 %collective-permute-start.1 = (bf16[12,1,4]{0,2,1:T(4,128)(2,1)S(1)}, bf16[12,1,4]{0,2,1:T(4,128)(2,1)S(1)}, u32[]{:S(2)}, u32[]{:S(2)}) collective-permute-start(bf16[12,1,4]{0,2,1:T(4,128)(2,1)S(1)} %bitcast.145), channel_id=1, source_target_pairs={{0,2},{2,0},{1,3},{3,1},{4,6},{6,4},{5,7},{7,5},{8,10},{10,8},{9,1... | collective-permute-start | bytes 296 | tf_op jit(solution)/shard_map/ppermute | solution.py:43
  55.9 6.9 %collective-permute-start = (bf16[12,1,4,1024]{3,2,0,1:T(4,128)(2,1)S(1)}, bf16[12,1,4,1024]{3,2,0,1:T(4,128)(2,1)S(1)}, u32[]{:S(2)}, u32[]{:S(2)}) collective-permute-start(bf16[12,1,4,1024]{3,2,0,1:T(4,128)(2,1)S(1)} %convert_bitcast_fusion), channel_id=1, source_target_pairs={{0,2},{2,0},{1,3},{3,1},{4,6},{6,4},{5,7},{7,5},{8,10},{10,8},{9,1... | collective-permute-start | bytes 294920 | tf_op jit(solution)/shard_map/ppermute | solution.py:43
  65.9 18.8 %copy-start.5 = (bf16[64,1024]{1,0:T(8,128)(2,1)S(1)}, bf16[64,1024]{1,0:T(8,128)(2,1)}, u32[]{:S(2)}) copy-start(bf16[64,1024]{1,0:T(8,128)(2,1)} %param.38) | copy-start | bytes 393220
  65.9 49.2 %copy-start.4 = (bf16[1,1024,128]{2,1,0:T(8,128)(2,1)S(1)}, bf16[1,1024,128]{2,1,0:T(8,128)(2,1)}, u32[]{:S(2)}) copy-start(bf16[1,1024,128]{2,1,0:T(8,128)(2,1)} %param.33) | copy-start | bytes 786436
  65.9 50.3 %copy-start.2 = (bf16[1,128,1024]{2,1,0:T(8,128)(2,1)S(1)}, bf16[1,128,1024]{2,1,0:T(8,128)(2,1)}, u32[]{:S(2)}) copy-start(bf16[1,128,1024]{2,1,0:T(8,128)(2,1)} %param.35) | copy-start | bytes 786436
  65.9 50.3 %copy-start.3 = (bf16[1,1024,128]{2,1,0:T(8,128)(2,1)S(1)}, bf16[1,1024,128]{2,1,0:T(8,128)(2,1)}, u32[]{:S(2)}) copy-start(bf16[1,1024,128]{2,1,0:T(8,128)(2,1)} %param.34) | copy-start | bytes 786436
  66.0 8.0 %collective-permute-start.2 = (f32[12,1,4]{0,2,1:T(4,128)S(1)}, f32[12,1,4]{0,2,1:T(4,128)S(1)}, u32[]{:S(2)}, u32[]{:S(2)}) collective-permute-start(f32[12,1,4]{0,2,1:T(4,128)S(1)} %bitcast.144), channel_id=1, source_target_pairs={{0,2},{2,0},{1,3},{3,1},{4,6},{6,4},{5,7},{7,5},{8,10},{10,8},{9,1... | collective-permute-start | bytes 584 | tf_op jit(solution)/shard_map/ppermute | solution.py:43
  75.1 8.8 %all-to-all-start.2 = ((bf16[4,12,1024]{2,1,0:T(8,128)(2,1)}), bf16[4,12,1024]{2,1,0:T(8,128)(2,1)S(1)}, u32[]{:S(2)}, u32[]{:S(2)}) async-start(bf16[4,12,1024]{2,1,0:T(8,128)(2,1)} %broadcast_in_dim.84), calls=%async_computation.2 | async-start | bytes 262144 | tf_op jit(solution)/shard_map/all_to_all | solution.py:21
  85.5 32.8 %all-to-all-start.6 = ((bf16[4,12,256]{2,1,0:T(8,128)(2,1)}), bf16[4,12,256]{2,1,0:T(8,128)(2,1)S(1)}, u32[]{:S(2)}, u32[]{:S(2)}) async-start(bf16[4,12,256]{2,1,0:T(8,128)(2,1)} %bitcast.135), calls=%async_computation.6 | async-start | bytes 65536 | tf_op jit(solution)/shard_map/all_to_all | solution.py:58
  118.3 10.0 %all-to-all-start.3 = ((bf16[4,128,256]{2,1,0:T(8,128)(2,1)}), bf16[4,128,256]{2,1,0:T(8,128)(2,1)S(1)}, u32[]{:S(2)}, u32[]{:S(2)}) async-start(bf16[4,128,256]{2,1,0:T(8,128)(2,1)} %bitcast.133), calls=%async_computation.3 | async-start | bytes 524288 | tf_op jit(solution)/shard_map/all_to_all | solution.py:58
